TPU v7x, 512 devices: a whole 4x4x16 slice. The times are simulated.
512 devices in a mesh: sp: 16 (over y, x), tp: 32 (over z, core).
Axes of the slice: x: 4, y: 4, z: 16, core: 2. Of those that a mesh axis runs over, the one named last changes fastest.
Arguments:
- tokens: bfloat16 [8, 49152, 2048], P(None, ('sp', 'tp')), may hold values from -13 to 13
- in_gain: float32 [2048], replicated, may hold values from 0.1 to 1.9
- w_key: bfloat16 [2048, 512], P('tp'), may hold values from -0.125 to 0.125
- w_value: bfloat16 [2048, 512], P('tp'), may hold values from -0.125 to 0.125
- k_gain: float32 [128], replicated, may hold values from 0.1 to 1.9
- new_query: bfloat16 [8, 1024], replicated, may hold values from -6 to 6
- q_gain: float32 [128], replicated, may hold values from 0.1 to 1.9
- stick_bias: float32 [8], replicated, may hold values from -13 to -3
Outputs:
- key_cache: bfloat16 [32, 49152, 128], P('tp', 'sp')
- value_cache: bfloat16 [32, 49152, 128], P('tp', 'sp')
- read_out: float32 [32, 256], P('tp')
All inputs are finite; a program needn't handle non-finite values.
Results may differ from a plain program's by a relative error of at most 0.005.
Values may be sent and summed in bfloat16 or wider, within the bound.
A program may use at most 64 MiB of HBM per device.

v0:
```python
import jax
import jax.numpy as jnp
from jax import lax
from jax.sharding import PartitionSpec as P

NORM_EPS = 1e-06


def in_one_piece(arrays, axis, dim, along):
    both = jnp.concatenate(arrays, axis=along)
    filled, at, outs = (lax.all_gather(both, axis, axis=dim, tiled=True), 0, [])
    for a in arrays:
        outs.append(lax.slice_in_dim(filled, at, at + a.shape[along], axis=along))
        at += a.shape[along]
    return tuple(outs)


def entering(value, axis, join, neutral):
    count, mine = (lax.axis_size(axis), lax.axis_index(axis))
    pieces = lax.all_gather(value, axis)
    pieces = pieces[::-1]
    mine = count - 1 - mine
    so_far = jnp.full_like(value, 0) + jnp.asarray(neutral, value.dtype)

    def turn(position, so_far):
        longer = join(so_far, pieces[position])
        return jnp.where(position < mine, longer, so_far)

    return lax.fori_loop(0, count - 1, turn, so_far)


def from_everyone(shard, axis):
    length = lax.axis_size(axis)
    return lax.all_to_all(
        jnp.broadcast_to(shard[None], (length, *shard.shape)), axis, 0, 0, tiled=True
    )


def of_everyone(shard, axis):
    everything = from_everyone(shard, axis)
    return jnp.sum(everything, axis=0)


def root_norm(values, scaling):
    inverse = lax.rsqrt(jnp.mean(values * values, axis=-1, keepdims=True) + NORM_EPS)
    return values * inverse * scaling


def add_later(earlier, later_part):
    return earlier + later_part


def shards(tokens, in_gain, w_key, w_value, k_gain, new_query, q_gain, stick_bias):
    seq_count, tok_seq, model_width = tokens.shape
    row_count = seq_count * tok_seq
    head_dim = k_gain.shape[0]
    kv_width = w_key.shape[1]
    kv_heads = kv_width // head_dim
    per_group = stick_bias.shape[0] // kv_heads
    inv_root = head_dim ** (-0.5)
    normed = root_norm(tokens.reshape(row_count, model_width).astype(jnp.float32), in_gain).astype(
        jnp.bfloat16
    )
    pieces = in_one_piece((w_key, w_value), "tp", 0, 1)
    key_raw = jnp.dot(normed, pieces[0], preferred_element_type=jnp.float32)
    value_raw = jnp.dot(normed, pieces[1], preferred_element_type=jnp.float32)
    key_rows = root_norm(key_raw.reshape(seq_count, tok_seq, kv_heads, head_dim), k_gain).astype(
        jnp.bfloat16
    )
    value_rows = value_raw.astype(jnp.bfloat16).reshape(seq_count, tok_seq, kv_heads, head_dim)
    query_rows = root_norm(
        new_query.astype(jnp.float32).reshape(seq_count, kv_heads, per_group, head_dim), q_gain
    ).astype(jnp.bfloat16)
    bias_rows = stick_bias.reshape(kv_heads, per_group)
    key_block = key_rows.transpose(2, 0, 1, 3).reshape(kv_heads * seq_count, tok_seq, head_dim)
    value_block = value_rows.transpose(2, 0, 1, 3).reshape(kv_heads * seq_count, tok_seq, head_dim)
    key_cache, value_cache = (
        lax.all_to_all(key_block, "tp", split_axis=0, concat_axis=1, tiled=True),
        lax.all_to_all(value_block, "tp", split_axis=0, concat_axis=1, tiled=True),
    )
    group_rows = key_cache.shape[0]
    row_start = lax.axis_index("tp") * group_rows
    query_flat = query_rows.transpose(1, 0, 2, 3).reshape(kv_heads * seq_count, per_group, head_dim)
    query_group = lax.dynamic_slice_in_dim(query_flat, row_start, group_rows, 0)
    bias_group = lax.dynamic_slice_in_dim(
        jnp.repeat(bias_rows, seq_count, axis=0), row_start, group_rows, 0
    )
    scores = (
        jnp.einsum("rqe,rpe->rqp", query_group, key_cache, preferred_element_type=jnp.float32)
        * inv_root
        + bias_group[:, :, None]
    )
    log_keep = jax.nn.log_sigmoid(-scores)
    log_total = jnp.sum(log_keep, axis=2)
    log_later = entering(log_total, "sp", add_later, jnp.zeros_like(log_total))
    log_after = log_later[:, :, None] + lax.cumsum(log_keep, axis=2, reverse=True) - log_keep
    weights = jnp.exp(jax.nn.log_sigmoid(scores) + log_after).astype(jnp.bfloat16)
    partial_value = jnp.einsum(
        "rqp,rpe->rqe", weights, value_cache, preferred_element_type=jnp.float32
    )
    read_out = of_everyone(partial_value.reshape(group_rows, per_group * head_dim), "sp")
    return (key_cache, value_cache, read_out)


def solution(mesh):
    return jax.shard_map(
        shards,
        mesh=mesh,
        in_specs=(
            P(None, ("sp", "tp"), None),
            P(),
            P("tp", None),
            P("tp", None),
            P(),
            P(),
            P(),
            P(),
        ),
        out_specs=(P("tp", "sp", None), P("tp", "sp", None), P("tp", None)),
        check_vma=False,
    )
```

profile of v0, /device:TPU:1, one launch (start us, length us, event | category | flops | bytes accessed | tf_op | source)
XLA Modules:
  0.0 228.2 jit_solution(18228065235646988775)
XLA Ops:
  7.2 1.5 pad_maximum_fusion
  8.8 2.6 %multiply_reduce_fusion = f32[8,96]{1,0:T(8,128)S(1)} fusion(bf16[8,96,2048]{2,1,0:T(8,128)(2,1)} %param.10), kind=kLoop, calls=%fused_computation.6 | loop fusion | flops 4717824 | bytes 3148800 | tf_op jit(solution)/shard_map/reduce_sum | solution.py:45
  11.4 78.4 %all-gather.3.cloned.1.call-done = bf16[2048,1024]{1,0:T(8,128)(2,1)} async-done(((bf16[64,1024]{1,0:T(8,128)(2,1)}), bf16[2048,1024]{1,0:T(8,128)(2,1)}) %all-gather.3.cloned.1.call-update) | async-done | bytes 4194320 | tf_op jit(solution)/shard_map/all_gather | solution.py:11
  89.7 3.1 %slice_bitcast_fusion = bf16[512,2048]{0,1:T(8,128)(2,1)} fusion(bf16[2048,1024]{1,0:T(8,128)(2,1)} %all-gather.3.cloned.1.call-done), kind=kLoop, calls=%fused_computation.16 | loop fusion | bytes 4194304 | tf_op jit(solution)/shard_map/dot_general | solution.py:65
  92.8 4.1 %copy.31 = bf16[512,2048]{1,0:T(8,128)(2,1)} copy(bf16[512,2048]{0,1:T(8,128)(2,1)} %slice_bitcast_fusion) | data formatting | bytes 4194304 | tf_op jit(solution)/shard_map/dot_general | solution.py:65
  97.0 3.9 %multiply_reduce_fusion.1 = (f32[8,96,4]{1,2,0:T(4,128)S(1)}, f32[8,96,4,128]{3,1,2,0:T(8,128)S(1)}) fusion(bf16[4,128,2048,1]{2,1,0,3:T(8,128)(2,1)} %bitcast.92, f32[2048]{0:T(1024)S(1)} %copy-done.3, f32[8,96]{1,0:T(8,128)S(1)} %add_rsqrt_fusion.1, bf16[8,96,2048]{2,1,0:T(8,128)(2,1)S(1)} %copy-done), kind=kOutput, calls=%fused_computation.20 | convolution fusion | flops 1617687552 | bytes 6839296 | tf_op jit(solution)/shard_map/dot_general | solution.py:65
  101.4 0.9 copy.32
  102.3 8.2 %all-to-all-start = ((bf16[32,96,128]{2,1,0:T(8,128)(2,1)}), bf16[32,96,128]{2,1,0:T(8,128)(2,1)}, u32[]{:S(2)}, u32[]{:S(2)}) async-start(bf16[32,96,128]{2,1,0:T(8,128)(2,1)} %bitcast.91), calls=%async_computation | async-start | bytes 1572864 | tf_op jit(solution)/shard_map/all_to_all | solution.py:78
  110.9 1.3 dynamic-slice
  113.2 0.8 fusion.1
  114.0 1.4 copy-done.1
  115.4 1.8 fusion.13
  117.4 1.0 copy.33
  118.4 36.7 %all-to-all-done = bf16[32,96,128]{2,1,0:T(8,128)(2,1)} async-done(((bf16[32,96,128]{2,1,0:T(8,128)(2,1)}), bf16[32,96,128]{2,1,0:T(8,128)(2,1)}, u32[]{:S(2)}, u32[]{:S(2)}) %all-to-all-start) | async-done | bytes 786464 | tf_op jit(solution)/shard_map/all_to_all | solution.py:78
  155.2 4.1 %all-to-all-start.1 = ((bf16[32,96,128]{2,1,0:T(8,128)(2,1)}), bf16[32,96,128]{2,1,0:T(8,128)(2,1)S(1)}, u32[]{:S(2)}, u32[]{:S(2)}) async-start(bf16[32,96,128]{2,1,0:T(8,128)(2,1)} %bitcast.11), calls=%async_computation.1 | async-start | bytes 1572864 | tf_op jit(solution)/shard_map/all_to_all | solution.py:79
  159.2 1.4 fusion.2
  161.0 34.8 %all-reduce = f32[32]{0:T(128)S(1)} all-reduce(f32[32]{0:T(128)S(1)} %negate_dynamic-update-slice_fusion), channel_id=2, replica_groups=mesh['sp'=16,'tp'=32] {'sp'}, use_global_device_ids=true, to_apply=%add | all-reduce | flops 32 | bytes 256
  195.9 2.5 %reduce-window.6 = f32[1,2,24,128]{3,2,1,0:T(8,128)S(1)} reduce-window(f32[1,2,24,128]{3,2,1,0:T(8,128)S(1)} %copy.58, f32[]{:T(128)} %constant.49.clone.1), window={size=1x1x1x128 pad=0_0x0_0x0_0x0_127}, to_apply=%region_6.7 | reduce-window | flops 780288 | bytes 49156 | tf_op jit(solution)/shard_map/reduce-window
  199.5 4.5 %all-to-all-done.1 = bf16[32,96,128]{2,1,0:T(8,128)(2,1)S(1)} async-done(((bf16[32,96,128]{2,1,0:T(8,128)(2,1)}), bf16[32,96,128]{2,1,0:T(8,128)(2,1)S(1)}, u32[]{:S(2)}, u32[]{:S(2)}) %all-to-all-start.1) | async-done | bytes 786464 | tf_op jit(solution)/shard_map/all_to_all | solution.py:79
  204.2 0.6 broadcast_in_dim.8
  204.9 6.5 %all-to-all-start.2 = ((f32[16,1,256]{2,1,0:T(1,128)}), f32[16,1,256]{2,1,0:T(1,128)S(1)}, u32[]{:S(2)}, u32[]{:S(2)}) async-start(f32[16,1,256]{2,1,0:T(1,128)} %broadcast_in_dim.8), calls=%async_computation.2 | async-start | bytes 32768 | tf_op jit(solution)/shard_map/all_to_all | solution.py:34
  211.4 6.4 %all-to-all-done.2 = f32[16,1,256]{2,1,0:T(1,128)S(1)} async-done(((f32[16,1,256]{2,1,0:T(1,128)}), f32[16,1,256]{2,1,0:T(1,128)S(1)}, u32[]{:S(2)}, u32[]{:S(2)}) %all-to-all-start.2) | async-done | bytes 16416 | tf_op jit(solution)/shard_map/all_to_all | solution.py:34
  218.4 2.1 copy.68
  220.5 0.9 copy.69
  (58 shorter events, 4.1 us)
Async XLA Ops:
  7.2 82.6 %all-gather.3.cloned.1.call-start = ((), (), s32[]{:S(2)}) async-start(), calls=%async_computation.3 | async-start | bytes 4325376 | tf_op jit(solution)/shard_map/all_gather | solution.py:11
  92.8 4.2 %copy-start = (bf16[8,96,2048]{2,1,0:T(8,128)(2,1)S(1)}, bf16[8,96,2048]{2,1,0:T(8,128)(2,1)}, u32[]{:S(2)}) copy-start(bf16[8,96,2048]{2,1,0:T(8,128)(2,1)} %param.10) | copy-start | bytes 9437188
  92.8 4.2 %copy-start.3 = (f32[2048]{0:T(1024)S(1)}, f32[2048]{0:T(1024)}, u32[]{:S(2)}) copy-start(f32[2048]{0:T(1024)} %param.11) | copy-start | bytes 24580
  97.0 3.9 %copy-start.6 = (f32[128]{0:T(128)S(1)}, f32[128]{0:T(128)}, u32[]{:S(2)}) copy-start(f32[128]{0:T(128)} %param.14) | copy-start | bytes 1540
  100.8 9.7 %copy-start.5 = (f32[8]{0:T(128)S(1)}, f32[8]{0:T(128)}, u32[]{:S(2)}) copy-start(f32[8]{0:T(128)} %param.17) | copy-start | bytes 100
  100.8 12.2 %copy-start.2 = (bf16[8,1024]{1,0:T(8,128)(2,1)S(1)}, bf16[8,1024]{1,0:T(8,128)(2,1)}, u32[]{:S(2)}) copy-start(bf16[8,1024]{1,0:T(8,128)(2,1)} %param.15) | copy-start | bytes 49156
  100.8 12.3 %copy-start.4 = (f32[128]{0:T(128)S(1)}, f32[128]{0:T(128)}, u32[]{:S(2)}) copy-start(f32[128]{0:T(128)} %param.16) | copy-start | bytes 1540
  102.3 52.8 %all-to-all-start = ((bf16[32,96,128]{2,1,0:T(8,128)(2,1)}), bf16[32,96,128]{2,1,0:T(8,128)(2,1)}, u32[]{:S(2)}, u32[]{:S(2)}) async-start(bf16[32,96,128]{2,1,0:T(8,128)(2,1)} %bitcast.91), calls=%async_computation | async-start | bytes 1572864 | tf_op jit(solution)/shard_map/all_to_all | solution.py:78
  113.2 2.2 copy-start.1
  155.2 48.8 %all-to-all-start.1 = ((bf16[32,96,128]{2,1,0:T(8,128)(2,1)}), bf16[32,96,128]{2,1,0:T(8,128)(2,1)S(1)}, u32[]{:S(2)}, u32[]{:S(2)}) async-start(bf16[32,96,128]{2,1,0:T(8,128)(2,1)} %bitcast.11), calls=%async_computation.1 | async-start | bytes 1572864 | tf_op jit(solution)/shard_map/all_to_all | solution.py:79
  204.9 13.0 %all-to-all-start.2 = ((f32[16,1,256]{2,1,0:T(1,128)}), f32[16,1,256]{2,1,0:T(1,128)S(1)}, u32[]{:S(2)}, u32[]{:S(2)}) async-start(f32[16,1,256]{2,1,0:T(1,128)} %broadcast_in_dim.8), calls=%async_computation.2 | async-start | bytes 32768 | tf_op jit(solution)/shard_map/all_to_all | solution.py:34
Sparse Core Ops, SparseCore 0:
  10.7 79.0 all-gather.2
where the time goes:
time: 229 us; the launch traced here: 228 us
  waiting for transfers between devices  126 us (55%)
  blocking collectives  34.8 us (15%)
  starting transfers between devices  18.8 us (8%)
  local copies, waits for them, and re-layouts  16.5 us (7%)
  between operations  14.9 us (7%)
  other arithmetic  9.44 us (4%)
  matrix products  7.38 us (3%)
    all_gather x1, waiting for transfers between devices, in_one_piece(): filled, at, outs = (lax.all_gather(both, axis, axis=dim, tiled=True), 0, [])  78.4 us
    all_to_all x1, waiting for transfers between devices, shards(): lax.all_to_all(key_block, 'tp', split_axis=0, concat_axis=1, tiled=True)  36.7 us
    unnamed x1, blocking collectives  34.8 us
    all_to_all x1, starting transfers between devices, shards(): lax.all_to_all(key_block, 'tp', split_axis=0, concat_axis=1, tiled=True)  8.16 us
    dot_general x2, local copies, waits for them, and re-layouts, shards(): key_raw = jnp.dot(normed, pieces[0], preferred_element_type=jnp.float32)  7.2 us
    all_to_all x1, starting transfers between devices, from_everyone(): lax.all_to_all(jnp.broadcast_to(shard[None], (length, *shard.shape)), axi...  6.53 us
    all_to_all x1, waiting for transfers between devices, from_everyone(): lax.all_to_all(jnp.broadcast_to(shard[None], (length, *shard.shape)), axi...  6.44 us
    unnamed x20, local copies, waits for them, and re-layouts  5.7 us
  transfers between devices with their start and end apart: 4, of which 4 were waited for; matrix products, arithmetic and copies ran while one was open for 6% of the time, Pallas kernels for 0%

commit v1 on v0

v1 whole, which is shorter than its diff:
```python
import functools

import jax
import jax.numpy as jnp
from jax import lax
from jax.experimental import pallas as pl
from jax.experimental.pallas import tpu as pltpu
from jax.sharding import PartitionSpec as P

MESH = pl.DeviceIdType.MESH
NORM_EPS = 1e-06
F32 = jnp.float32
BF16 = jnp.bfloat16

Z = 16
SIDE = 4
SEQS = 8
TOK = 96
PAIR = 2 * TOK
D = 2048
HD = 128
SPAN = Z * PAIR
CHUNKS = SPAN // HD


def log1p_unit(e):
    t = e / (2.0 + e)
    t2 = t * t
    acc = jnp.full_like(t, 1.0 / 15.0)
    for n in (13.0, 11.0, 9.0, 7.0, 5.0, 3.0):
        acc = acc * t2 + 1.0 / n
    return 2.0 * t * (acc * t2 + 1.0)


def far_first(i):
    return Z // 2 + (1 - 2 * (i % 2)) * ((i + 1) // 2)


def kernel(
    tokens_ref, in_gain_ref, w_key_ref, w_value_ref, k_gain_ref, query_ref, q_gain_ref, bias_ref,
    key_out, value_out, read_out,
    raw, normed, weights, sendbuf, kv, scores, queries, qflat, parts,
    tok_sem, wz_send, wz_recv, wl_sem, w1_send, w1_recv, w2_send, w2_recv, x_send, x_recv,
    kv_send, kv_recv, out_sem, p_send, p_recv,
):
    sp = lax.axis_index("sp")
    tp = lax.axis_index("tp")
    z, core = tp // 2, tp % 2
    y, x = sp // SIDE, sp % SIDE
    first, second = y + core * (x - y), x + core * (y - x)
    first_step, second_step = SIDE - 3 * core, 1 + 3 * core

    barrier = pltpu.get_barrier_semaphore()

    def greet_tp(i, carry):
        pl.semaphore_signal(barrier, inc=1, device_id=(sp, (tp + i) % (2 * Z)), device_id_type=MESH)
        return carry

    def greet_sp(i, carry):
        pl.semaphore_signal(barrier, inc=1, device_id=((sp + i) % (SIDE * SIDE), tp), device_id_type=MESH)
        return carry

    lax.fori_loop(1, 2 * Z, greet_tp, 0)
    lax.fori_loop(1, SIDE * SIDE, greet_sp, 0)

    def fetch(s, carry):
        pltpu.make_async_copy(tokens_ref.at[s], raw.at[s], tok_sem.at[s]).start()
        return carry

    lax.fori_loop(0, SEQS, fetch, 0)

    for i in range(8):
        qflat[i] = query_ref[:, pl.ds(i * HD, HD)].astype(F32)
    group, seq = tp // SEQS, tp % SEQS
    queries[...] = jnp.zeros_like(queries)
    for i in range(2):
        head = qflat[group * 2 + i, pl.ds(seq, 1), :]
        inverse = lax.rsqrt(jnp.mean(head * head, axis=-1, keepdims=True) + NORM_EPS)
        queries[pl.ds(i, 1), :] = head * inverse * q_gain_ref[...]

    pl.semaphore_wait(barrier, 2 * Z - 1 + SIDE * SIDE - 1)

    def tile_of(target_core, to_z):
        ref = (w_key_ref, w_value_ref)[target_core]
        rows, cols = ((y, x), (x, y))[target_core]
        return ref.at[pl.ds(pl.multiple_of(rows * 16, 16), 16), pl.ds(pl.multiple_of((cols + to_z) % SIDE * HD, HD), HD)]

    def landing(target_core):
        return weights.at[0, tp, (y, x)[target_core]]

    def deal(i, carry):
        to_z = (z + far_first(i)) % Z
        for target_core in range(2):
            pltpu.make_async_remote_copy(
                tile_of(target_core, to_z), landing(target_core), wz_send, wz_recv,
                device_id=(sp, to_z * 2 + target_core), device_id_type=MESH,
            ).start()
        return carry

    lax.fori_loop(0, Z - 1, deal, 0)
    for target_core in range(2):
        @pl.when(core == target_core)
        def _():
            pltpu.make_async_copy(tile_of(target_core, z), landing(target_core), wl_sem).start()

        @pl.when(core != target_core)
        def _():
            pltpu.make_async_remote_copy(
                tile_of(target_core, z), landing(target_core), wz_send, wz_recv,
                device_id=(sp, z * 2 + target_core), device_id_type=MESH,
            ).start()

    def norm(s, carry):
        pltpu.make_async_copy(tokens_ref.at[s], raw.at[s], tok_sem.at[s]).wait()
        for part in range(TOK // 16):
            rows = raw[s, pl.ds(part * 16, 16), :].astype(F32)
            inverse = lax.rsqrt(jnp.mean(rows * rows, axis=-1, keepdims=True) + NORM_EPS)
            normed[s, core, pl.ds(part * 16, 16), :] = (rows * inverse * in_gain_ref[...]).astype(BF16)
        pltpu.make_async_remote_copy(
            normed.at[s, core], normed.at[s, core], x_send, x_recv,
            device_id=(sp, z * 2 + 1 - core), device_id_type=MESH,
        ).start()
        return carry

    lax.fori_loop(0, SEQS, norm, 0)

    def sp_of(a, b):
        return a * first_step + b * second_step

    pltpu.make_async_copy(landing(0), landing(0), wl_sem).wait()
    column = weights.at[0, pl.ds(0, 2 * Z - 1), 0]
    pltpu.make_async_copy(column, column, wz_recv).wait()
    strip = weights.at[0, :, first]
    for i in (1, 3, 2):
        pltpu.make_async_remote_copy(
            strip, strip, w1_send, w1_recv,
            device_id=(sp_of((first + i) % SIDE, second), tp), device_id_type=MESH,
        ).start()
    three = weights.at[0, :, pl.ds(0, 3)]
    pltpu.make_async_copy(three, three, w1_recv).wait()
    for i in (1, 3, 2):
        pltpu.make_async_remote_copy(
            weights.at[0], weights.at[i], w2_send, w2_recv.at[i],
            device_id=(sp_of(first, (second + SIDE - i) % SIDE), tp), device_id_type=MESH,
        ).start()

    half = normed.at[:, 0]
    pltpu.make_async_copy(half, half, x_recv).wait()

    for slot in (0, 1, 3, 2):
        if slot:
            pltpu.make_async_copy(weights.at[slot], weights.at[slot], w2_recv.at[slot]).wait()
        head = (second + slot + z) % SIDE

        def project(s, carry):
            raw_rows = jnp.dot(
                normed[s].reshape(PAIR, D), weights[slot].reshape(D, HD), preferred_element_type=F32
            )
            inverse = lax.rsqrt(jnp.mean(raw_rows * raw_rows, axis=-1, keepdims=True) + NORM_EPS)
            out = jnp.where(core == 0, raw_rows * inverse * k_gain_ref[...], raw_rows)
            sendbuf[slot * SEQS + s] = out.astype(BF16)
            target = head * SEQS + s
            source = sendbuf.at[slot * SEQS + s]
            there = kv.at[core, pl.ds(pl.multiple_of(z * PAIR, PAIR), PAIR)]

            @pl.when(target == tp)
            def _():
                pltpu.make_async_copy(source, there, kv_recv.at[core, z]).start()

            @pl.when(target != tp)
            def _():
                pltpu.make_async_remote_copy(
                    source, there, kv_send, kv_recv.at[core, z],
                    device_id=(sp, target), device_id_type=MESH,
                ).start()

            return carry

        lax.fori_loop(0, SEQS, project, 0)

    query = queries[...].astype(BF16)

    def score(pair, carry):
        for i in range(2):
            at = pair * 2 + i
            block = kv.at[0, pl.ds(pl.multiple_of(at * PAIR, PAIR), PAIR)]
            pltpu.make_async_copy(block, block, kv_recv.at[0, at]).wait()
        for i in range(3):
            chunk = pair * 3 + i
            keys = kv[0, pl.ds(pl.multiple_of(chunk * HD, HD), HD), :]
            scores[chunk] = lax.dot_general(query, keys, (((1,), (1,)), ((), ())), preferred_element_type=F32)[:8]
        span = pl.ds(pl.multiple_of(pair * 2 * PAIR, 2 * PAIR), 2 * PAIR)
        pltpu.make_async_copy(kv.at[0, span], key_out.at[0, span], out_sem).start()
        return carry

    lax.fori_loop(0, Z // 2, score, 0)

    row = lax.broadcasted_iota(jnp.int32, (1, 8, HD), 1)
    bias = jnp.where(row == 0, bias_ref[group * 2], bias_ref[group * 2 + 1])
    score_all = scores[...] * (HD ** -0.5) + bias
    soft = log1p_unit(jnp.exp(-jnp.abs(score_all)))
    log_keep = -(jnp.maximum(score_all, 0.0) + soft)
    log_take = -(jnp.maximum(-score_all, 0.0) + soft)
    later = (
        lax.broadcasted_iota(jnp.int32, (HD, HD), 0) > lax.broadcasted_iota(jnp.int32, (HD, HD), 1)
    ).astype(F32)
    after = jnp.dot(
        log_keep.reshape(CHUNKS * 8, HD), later, preferred_element_type=F32, precision=lax.Precision.HIGHEST
    ).reshape(CHUNKS, 8, HD)
    totals = jnp.sum(log_keep, axis=2, keepdims=True)
    carried = jnp.zeros((8, 1), F32)
    chunk_weights = [None] * CHUNKS
    for chunk in reversed(range(CHUNKS)):
        chunk_weights[chunk] = jnp.exp(log_take[chunk] + after[chunk] + carried).astype(BF16)
        carried = carried + totals[chunk]

    def arrive(at, carry):
        block = kv.at[1, pl.ds(pl.multiple_of(at * PAIR, PAIR), PAIR)]
        pltpu.make_async_copy(block, block, kv_recv.at[1, at]).wait()
        return carry

    lax.fori_loop(0, Z, arrive, 0)
    pltpu.make_async_copy(kv.at[1], value_out.at[0], out_sem).start()
    partial = jnp.zeros((8, HD), F32)
    for chunk in range(CHUNKS):
        partial = partial + jnp.dot(
            chunk_weights[chunk], kv[1, pl.ds(chunk * HD, HD), :], preferred_element_type=F32
        )

    parts[sp, pl.ds(0, 8), :] = partial
    parts[sp, pl.ds(8, 8), :] = jnp.broadcast_to(carried, (8, HD))

    def share(i, carry):
        pltpu.make_async_remote_copy(
            parts.at[sp], parts.at[sp], p_send, p_recv,
            device_id=((sp + i) % (SIDE * SIDE), tp), device_id_type=MESH,
        ).start()
        return carry

    lax.fori_loop(1, SIDE * SIDE, share, 0)
    others = parts.at[pl.ds(0, SIDE * SIDE - 1)]
    pltpu.make_async_copy(others, others, p_recv).wait()
    total = jnp.zeros((8, HD), F32)
    log_later = jnp.zeros((8, HD), F32)
    for span in reversed(range(SIDE * SIDE)):
        total = total + jnp.exp(log_later) * parts[span, pl.ds(0, 8), :]
        log_later = log_later + parts[span, pl.ds(8, 8), :]
    read_out[:, pl.ds(0, HD)] = total[0:1]
    read_out[:, pl.ds(HD, HD)] = total[1:2]

    pltpu.make_async_copy(column, column, wz_send).wait()
    pltpu.make_async_copy(three, three, w1_send).wait()
    pltpu.make_async_copy(weights.at[pl.ds(0, 3)], weights.at[pl.ds(0, 3)], w2_send).wait()
    pltpu.make_async_copy(half, half, x_send).wait()

    sent = sendbuf.at[pl.ds(0, 2 * Z - 1)]
    pltpu.make_async_copy(sent, sent, kv_send).wait()
    pltpu.make_async_copy(others, others, p_send).wait()
    pltpu.make_async_copy(kv.at[0], key_out.at[0], out_sem).wait()
    pltpu.make_async_copy(kv.at[1], value_out.at[0], out_sem).wait()


def shards(tokens, in_gain, w_key, w_value, k_gain, new_query, q_gain, stick_bias):
    vmem = pl.BlockSpec(memory_space=pltpu.VMEM)
    hbm = pl.BlockSpec(memory_space=pl.ANY)
    dma = pltpu.SemaphoreType.DMA
    return pl.pallas_call(
        kernel,
        out_shape=(
            jax.ShapeDtypeStruct((1, SPAN, HD), BF16),
            jax.ShapeDtypeStruct((1, SPAN, HD), BF16),
            jax.ShapeDtypeStruct((1, 2 * HD), F32),
        ),
        in_specs=[hbm, vmem, vmem, vmem, vmem, vmem, vmem, pl.BlockSpec(memory_space=pltpu.SMEM)],
        out_specs=(hbm, hbm, vmem),
        scratch_shapes=[
            pltpu.VMEM((SEQS, TOK, D), BF16),
            pltpu.VMEM((SEQS, 2, TOK, D), BF16),
            pltpu.VMEM((SIDE, 2 * Z, 4, 16, HD), BF16),
            pltpu.VMEM((2 * Z, PAIR, HD), BF16),
            pltpu.VMEM((2, SPAN, HD), BF16),
            pltpu.VMEM((CHUNKS, 8, HD), F32),
            pltpu.VMEM((16, HD), F32),
            pltpu.VMEM((8, SEQS, HD), F32),
            pltpu.VMEM((SIDE * SIDE, 16, HD), F32),
            dma((SEQS,)), dma, dma, dma, dma, dma, dma, dma((SIDE,)), dma, dma,
            dma, dma((2, Z)), dma, dma, dma,
        ],
        compiler_params=pltpu.CompilerParams(
            collective_id=0, has_side_effects=True, vmem_limit_bytes=40 * 2**20
        ),
    )(
        tokens, in_gain.reshape(1, D), w_key, w_value, k_gain.reshape(1, HD), new_query,
        q_gain.reshape(1, HD), stick_bias,
    )


def solution(mesh):
    return jax.shard_map(
        shards,
        mesh=mesh,
        in_specs=(
            P(None, ("sp", "tp"), None), P(), P("tp", None), P("tp", None), P(), P(), P(), P(),
        ),
        out_specs=(P("tp", "sp", None), P("tp", "sp", None), P("tp", None)),
        check_vma=False,
    )
```

time: 229 us -> 125 us (0.55)
  the two profiles are of different devices: /device:TPU:1 before, /device:TPU:97 now
where the time goes in v1:
time: 125 us
  Pallas kernels  115 us (92%)
  local copies, waits for them, and re-layouts  9.26 us (7%)
    pallas_call x1, Pallas kernels, shards(): pl.pallas_call(kernel, out_shape=(jax.ShapeDtypeStruct((1, SPAN, HD), BF1...  115 us
    unnamed x19, local copies, waits for them, and re-layouts  9.26 us

profile of v1, /device:TPU:97, one launch (start us, length us, event | category | flops | bytes accessed | tf_op | source)
XLA Modules:
  0.0 124.8 jit_solution(17291585307826728100)
XLA Ops:
  0.6 0.0 copy-start
  0.6 1.9 %copy-done = bf16[8,96,2048]{2,1,0:T(8,128)(2,1)S(1)} copy-done((bf16[8,96,2048]{2,1,0:T(8,128)(2,1)S(1)}, bf16[8,96,2048]{2,1,0:T(8,128)(2,1)}, u32[]{:S(2)}) %copy-start) | copy-done | bytes 3145752
  2.5 0.0 copy-start.1
  2.5 0.8 copy-done.1
  3.4 0.0 copy-start.2
  3.4 0.8 copy-done.2
  4.2 0.0 copy-start.3
  4.2 0.7 copy-done.3
  4.9 0.0 copy-start.4
  4.9 0.7 copy-done.4
  5.6 0.0 copy-start.5
  5.6 0.7 copy-done.5
  6.3 0.0 copy-start.6
  6.3 0.7 copy-done.6
  6.9 0.0 copy-start.7
  6.9 0.7 copy-done.7
  7.6 114.8 %shard_map.103 = (bf16[1,3072,128]{2,1,0:T(8,128)(2,1)S(1)}, bf16[1,3072,128]{2,1,0:T(8,128)(2,1)S(1)}, f32[1,256]{1,0:T(1,128)S(1)}) custom-call(bf16[8,96,2048]{2,1,0:T(8,128)(2,1)S(1)} %copy-done, f32[1,2048]{1,0:T(1,128)S(1)} %bitcast.3, bf16[64,512]{1,0:T(8,128)(2,1)S(1)} %copy-done.1, bf16[64,512]{1,0:T(8,128)(2,1)S(1)} %copy-done.2, ...), custom_call_target="tpu_custom_call" | custom-call | tf_op jit(solution)/shard_map/pallas_call | solution.py:267
  122.4 0.9 copy.14
  123.3 0.9 copy.15
  124.2 0.6 copy.16
Async XLA Ops:
  0.6 1.9 %copy-start = (bf16[8,96,2048]{2,1,0:T(8,128)(2,1)S(1)}, bf16[8,96,2048]{2,1,0:T(8,128)(2,1)}, u32[]{:S(2)}) copy-start(bf16[8,96,2048]{2,1,0:T(8,128)(2,1)} %tokens_ref.1) | copy-start | bytes 9437188
  2.5 0.8 copy-start.1
  3.4 0.8 copy-start.2
  4.2 0.7 copy-start.3
  4.9 0.7 copy-start.4
  5.6 0.7 copy-start.5
  6.3 0.7 copy-start.6
  6.9 0.7 copy-start.7

commit v2 on v1

--- a/solution.py
+++ b/solution.py
@@ -37,11 +37,12 @@
 
 
 def kernel(
-    tokens_ref, in_gain_ref, w_key_ref, w_value_ref, k_gain_ref, query_ref, q_gain_ref, bias_ref,
+    tokens_ref, in_gain_in, w_key_in, w_value_in, k_gain_in, query_in, q_gain_in, bias_in,
     key_out, value_out, read_out,
-    raw, normed, weights, sendbuf, kv, scores, queries, qflat, parts,
-    tok_sem, wz_send, wz_recv, wl_sem, w1_send, w1_recv, w2_send, w2_recv, x_send, x_recv,
-    kv_send, kv_recv, out_sem, p_send, p_recv,
+    in_gain_ref, w_key_ref, w_value_ref, k_gain_ref, query_ref, q_gain_ref, bias_ref,
+    raw, normed, weights, sendbuf, scores, queries, qflat, parts,
+    in_sem, tok_sem, wz_send, wz_recv, wl_sem, w1_send, w1_recv, w2_send, w2_recv, x_send, x_recv,
+    kv_send, kv_recv, p_send, p_recv,
 ):
     sp = lax.axis_index("sp")
     tp = lax.axis_index("tp")
@@ -63,11 +64,24 @@
     lax.fori_loop(1, 2 * Z, greet_tp, 0)
     lax.fori_loop(1, SIDE * SIDE, greet_sp, 0)
 
+    fetched = [
+        pltpu.make_async_copy(source, target, in_sem.at[i])
+        for i, (source, target) in enumerate((
+            (w_key_in, w_key_ref), (w_value_in, w_value_ref), (query_in, query_ref), (q_gain_in, q_gain_ref),
+            (in_gain_in, in_gain_ref), (k_gain_in, k_gain_ref), (bias_in, bias_ref),
+        ))
+    ]
+    for copy in fetched:
+        copy.start()
+
     def fetch(s, carry):
         pltpu.make_async_copy(tokens_ref.at[s], raw.at[s], tok_sem.at[s]).start()
         return carry
 
     lax.fori_loop(0, SEQS, fetch, 0)
+
+    for copy in fetched:
+        copy.wait()
 
     for i in range(8):
         qflat[i] = query_ref[:, pl.ds(i * HD, HD)].astype(F32)
@@ -78,7 +92,8 @@
         inverse = lax.rsqrt(jnp.mean(head * head, axis=-1, keepdims=True) + NORM_EPS)
         queries[pl.ds(i, 1), :] = head * inverse * q_gain_ref[...]
 
-    pl.semaphore_wait(barrier, 2 * Z - 1 + SIDE * SIDE - 1)
+    with jax.named_scope("barrier"):
+        pl.semaphore_wait(barrier, 2 * Z - 1 + SIDE * SIDE - 1)
 
     def tile_of(target_core, to_z):
         ref = (w_key_ref, w_value_ref)[target_core]
@@ -97,7 +112,8 @@
             ).start()
         return carry
 
-    lax.fori_loop(0, Z - 1, deal, 0)
+    with jax.named_scope("deal"):
+        lax.fori_loop(0, Z - 1, deal, 0)
     for target_core in range(2):
         @pl.when(core == target_core)
         def _():
@@ -122,14 +138,16 @@
         ).start()
         return carry
 
-    lax.fori_loop(0, SEQS, norm, 0)
+    with jax.named_scope("norm"):
+        lax.fori_loop(0, SEQS, norm, 0)
 
     def sp_of(a, b):
         return a * first_step + b * second_step
 
     pltpu.make_async_copy(landing(0), landing(0), wl_sem).wait()
     column = weights.at[0, pl.ds(0, 2 * Z - 1), 0]
-    pltpu.make_async_copy(column, column, wz_recv).wait()
+    with jax.named_scope("z_phase"):
+        pltpu.make_async_copy(column, column, wz_recv).wait()
     strip = weights.at[0, :, first]
     for i in (1, 3, 2):
         pltpu.make_async_remote_copy(
@@ -137,7 +155,8 @@
             device_id=(sp_of((first + i) % SIDE, second), tp), device_id_type=MESH,
         ).start()
     three = weights.at[0, :, pl.ds(0, 3)]
-    pltpu.make_async_copy(three, three, w1_recv).wait()
+    with jax.named_scope("first_phase"):
+        pltpu.make_async_copy(three, three, w1_recv).wait()
     for i in (1, 3, 2):
         pltpu.make_async_remote_copy(
             weights.at[0], weights.at[i], w2_send, w2_recv.at[i],
@@ -145,11 +164,13 @@
         ).start()
 
     half = normed.at[:, 0]
-    pltpu.make_async_copy(half, half, x_recv).wait()
+    with jax.named_scope("partner"):
+        pltpu.make_async_copy(half, half, x_recv).wait()
 
     for slot in (0, 1, 3, 2):
         if slot:
-            pltpu.make_async_copy(weights.at[slot], weights.at[slot], w2_recv.at[slot]).wait()
+            with jax.named_scope("slot"):
+                pltpu.make_async_copy(weights.at[slot], weights.at[slot], w2_recv.at[slot]).wait()
         head = (second + slot + z) % SIDE
 
         def project(s, carry):
@@ -161,39 +182,40 @@
             sendbuf[slot * SEQS + s] = out.astype(BF16)
             target = head * SEQS + s
             source = sendbuf.at[slot * SEQS + s]
-            there = kv.at[core, pl.ds(pl.multiple_of(z * PAIR, PAIR), PAIR)]
-
-            @pl.when(target == tp)
-            def _():
-                pltpu.make_async_copy(source, there, kv_recv.at[core, z]).start()
-
-            @pl.when(target != tp)
-            def _():
-                pltpu.make_async_remote_copy(
-                    source, there, kv_send, kv_recv.at[core, z],
-                    device_id=(sp, target), device_id_type=MESH,
-                ).start()
+            for which, out_ref in enumerate((key_out, value_out)):
+                there = out_ref.at[0, pl.ds(pl.multiple_of(z * PAIR, PAIR), PAIR)]
+
+                @pl.when(jnp.logical_and(core == which, target == tp))
+                def _():
+                    pltpu.make_async_copy(source, there, kv_recv.at[which, z]).start()
+
+                @pl.when(jnp.logical_and(core == which, target != tp))
+                def _():
+                    pltpu.make_async_remote_copy(
+                        source, there, kv_send, kv_recv.at[which, z],
+                        device_id=(sp, target), device_id_type=MESH,
+                    ).start()
 
             return carry
 
-        lax.fori_loop(0, SEQS, project, 0)
+        with jax.named_scope("project"):
+            lax.fori_loop(0, SEQS, project, 0)
 
     query = queries[...].astype(BF16)
 
     def score(pair, carry):
         for i in range(2):
             at = pair * 2 + i
-            block = kv.at[0, pl.ds(pl.multiple_of(at * PAIR, PAIR), PAIR)]
+            block = key_out.at[0, pl.ds(pl.multiple_of(at * PAIR, PAIR), PAIR)]
             pltpu.make_async_copy(block, block, kv_recv.at[0, at]).wait()
         for i in range(3):
             chunk = pair * 3 + i
-            keys = kv[0, pl.ds(pl.multiple_of(chunk * HD, HD), HD), :]
+            keys = key_out[0, pl.ds(pl.multiple_of(chunk * HD, HD), HD), :]
             scores[chunk] = lax.dot_general(query, keys, (((1,), (1,)), ((), ())), preferred_element_type=F32)[:8]
-        span = pl.ds(pl.multiple_of(pair * 2 * PAIR, 2 * PAIR), 2 * PAIR)
-        pltpu.make_async_copy(kv.at[0, span], key_out.at[0, span], out_sem).start()
-        return carry
-
-    lax.fori_loop(0, Z // 2, score, 0)
+        return carry
+
+    with jax.named_scope("score"):
+        lax.fori_loop(0, Z // 2, score, 0)
 
     row = lax.broadcasted_iota(jnp.int32, (1, 8, HD), 1)
     bias = jnp.where(row == 0, bias_ref[group * 2], bias_ref[group * 2 + 1])
@@ -215,16 +237,16 @@
         carried = carried + totals[chunk]
 
     def arrive(at, carry):
-        block = kv.at[1, pl.ds(pl.multiple_of(at * PAIR, PAIR), PAIR)]
+        block = value_out.at[0, pl.ds(pl.multiple_of(at * PAIR, PAIR), PAIR)]
         pltpu.make_async_copy(block, block, kv_recv.at[1, at]).wait()
         return carry
 
-    lax.fori_loop(0, Z, arrive, 0)
-    pltpu.make_async_copy(kv.at[1], value_out.at[0], out_sem).start()
+    with jax.named_scope("arrive"):
+        lax.fori_loop(0, Z, arrive, 0)
     partial = jnp.zeros((8, HD), F32)
     for chunk in range(CHUNKS):
         partial = partial + jnp.dot(
-            chunk_weights[chunk], kv[1, pl.ds(chunk * HD, HD), :], preferred_element_type=F32
+            chunk_weights[chunk], value_out[0, pl.ds(chunk * HD, HD), :], preferred_element_type=F32
         )
 
     parts[sp, pl.ds(0, 8), :] = partial
@@ -239,7 +261,8 @@
 
     lax.fori_loop(1, SIDE * SIDE, share, 0)
     others = parts.at[pl.ds(0, SIDE * SIDE - 1)]
-    pltpu.make_async_copy(others, others, p_recv).wait()
+    with jax.named_scope("others"):
+        pltpu.make_async_copy(others, others, p_recv).wait()
     total = jnp.zeros((8, HD), F32)
     log_later = jnp.zeros((8, HD), F32)
     for span in reversed(range(SIDE * SIDE)):
@@ -254,15 +277,14 @@
     pltpu.make_async_copy(half, half, x_send).wait()
 
     sent = sendbuf.at[pl.ds(0, 2 * Z - 1)]
-    pltpu.make_async_copy(sent, sent, kv_send).wait()
+    with jax.named_scope("drain"):
+        pltpu.make_async_copy(sent, sent, kv_send).wait()
     pltpu.make_async_copy(others, others, p_send).wait()
-    pltpu.make_async_copy(kv.at[0], key_out.at[0], out_sem).wait()
-    pltpu.make_async_copy(kv.at[1], value_out.at[0], out_sem).wait()
 
 
 def shards(tokens, in_gain, w_key, w_value, k_gain, new_query, q_gain, stick_bias):
     vmem = pl.BlockSpec(memory_space=pltpu.VMEM)
-    hbm = pl.BlockSpec(memory_space=pl.ANY)
+    hbm = pl.BlockSpec(memory_space=pltpu.HBM)
     dma = pltpu.SemaphoreType.DMA
     return pl.pallas_call(
         kernel,
@@ -271,27 +293,38 @@
             jax.ShapeDtypeStruct((1, SPAN, HD), BF16),
             jax.ShapeDtypeStruct((1, 2 * HD), F32),
         ),
-        in_specs=[hbm, vmem, vmem, vmem, vmem, vmem, vmem, pl.BlockSpec(memory_space=pltpu.SMEM)],
-        out_specs=(hbm, hbm, vmem),
+        in_specs=[hbm] * 8,
+        out_specs=(vmem, vmem, vmem),
         scratch_shapes=[
+            pltpu.VMEM((1, D), F32),
+            pltpu.VMEM(w_key.shape, BF16),
+            pltpu.VMEM(w_value.shape, BF16),
+            pltpu.VMEM((1, HD), F32),
+            pltpu.VMEM(new_query.shape, BF16),
+            pltpu.VMEM((1, HD), F32),
+            pltpu.SMEM(stick_bias.shape, F32),
             pltpu.VMEM((SEQS, TOK, D), BF16),
             pltpu.VMEM((SEQS, 2, TOK, D), BF16),
             pltpu.VMEM((SIDE, 2 * Z, 4, 16, HD), BF16),
             pltpu.VMEM((2 * Z, PAIR, HD), BF16),
-            pltpu.VMEM((2, SPAN, HD), BF16),
             pltpu.VMEM((CHUNKS, 8, HD), F32),
             pltpu.VMEM((16, HD), F32),
             pltpu.VMEM((8, SEQS, HD), F32),
             pltpu.VMEM((SIDE * SIDE, 16, HD), F32),
-            dma((SEQS,)), dma, dma, dma, dma, dma, dma, dma((SIDE,)), dma, dma,
-            dma, dma((2, Z)), dma, dma, dma,
+            dma((7,)), dma((SEQS,)), dma, dma, dma, dma, dma, dma, dma((SIDE,)), dma, dma,
+            dma, dma((2, Z)), dma, dma,
         ],
         compiler_params=pltpu.CompilerParams(
             collective_id=0, has_side_effects=True, vmem_limit_bytes=40 * 2**20
         ),
     )(
-        tokens, in_gain.reshape(1, D), w_key, w_value, k_gain.reshape(1, HD), new_query,
-        q_gain.reshape(1, HD), stick_bias,
+        *(
+            pltpu.with_memory_space_constraint(a, pltpu.HBM)
+            for a in (
+                tokens, in_gain.reshape(1, D), w_key, w_value, k_gain.reshape(1, HD), new_query,
+                q_gain.reshape(1, HD), stick_bias,
+            )
+        )
     )
 
 

time: 125 us -> 117 us (0.936)
  local copies, waits for them, and re-layouts: 9.26 us -> 2.32 us
    unnamed x19 -> x3, local copies, waits for them, and re-layouts: 9.26 us -> 2.32 us
where the time goes in v2:
time: 117 us
  Pallas kernels  114 us (97%)
  local copies, waits for them, and re-layouts  2.32 us (2%)
    pallas_call x1, Pallas kernels, shards(): pl.pallas_call(kernel, out_shape=(jax.ShapeDtypeStruct((1, SPAN, HD), BF1...  114 us

profile of v2, /device:TPU:97, one launch (start us, length us, event | category | flops | bytes accessed | tf_op | source)
XLA Modules:
  0.0 116.9 jit_solution(14667395657054726802)
XLA Ops:
  0.6 114.0 %shard_map.103 = (bf16[1,3072,128]{2,1,0:T(8,128)(2,1)S(1)}, bf16[1,3072,128]{2,1,0:T(8,128)(2,1)S(1)}, f32[1,256]{1,0:T(1,128)S(1)}) custom-call(bf16[8,96,2048]{2,1,0:T(8,128)(2,1)} %tokens_ref.1, f32[1,2048]{1,0:T(1,128)} %bitcast.3, bf16[64,512]{1,0:T(8,128)(2,1)} %w_key_in.1, bf16[64,512]{1,0:T(8,128)(2,1)} %w_value_in.1, f32[1,128]{1,0:T(1,128)} %bitcast.4, ...), custom_call_target="tpu_custom_call" | custom-call | tf_op jit(solution)/shard_map/pallas_call | solution.py:289
  114.6 0.9 copy.14
  115.5 0.9 copy.15
  116.4 0.6 copy.16

commit v3 on v2

--- a/solution.py
+++ b/solution.py
@@ -32,15 +32,23 @@
     return 2.0 * t * (acc * t2 + 1.0)
 
 
+def turn(target_core, chip_z):
+    return chip_z // SIDE + (chip_z + target_core * (Z - 2 * chip_z))
+
+
+def half_of(slot):
+    return 0 if slot == 1 else Z
+
+
 def far_first(i):
     return Z // 2 + (1 - 2 * (i % 2)) * ((i + 1) // 2)
 
 
 def kernel(
     tokens_ref, in_gain_in, w_key_in, w_value_in, k_gain_in, query_in, q_gain_in, bias_in,
-    key_out, value_out, read_out,
+    key_out, value_out, parts,
     in_gain_ref, w_key_ref, w_value_ref, k_gain_ref, query_ref, q_gain_ref, bias_ref,
-    raw, normed, weights, sendbuf, scores, queries, qflat, parts,
+    raw, normed, weights, sendbuf, scores, queries, qflat,
     in_sem, tok_sem, wz_send, wz_recv, wl_sem, w1_send, w1_recv, w2_send, w2_recv, x_send, x_recv,
     kv_send, kv_recv, p_send, p_recv,
 ):
@@ -90,7 +98,9 @@
     for i in range(2):
         head = qflat[group * 2 + i, pl.ds(seq, 1), :]
         inverse = lax.rsqrt(jnp.mean(head * head, axis=-1, keepdims=True) + NORM_EPS)
-        queries[pl.ds(i, 1), :] = head * inverse * q_gain_ref[...]
+        head = head * inverse * q_gain_ref[...]
+        queries[pl.ds(i, 1), :] = head
+        queries[pl.ds(i + 2, 1), :] = head
 
     with jax.named_scope("barrier"):
         pl.semaphore_wait(barrier, 2 * Z - 1 + SIDE * SIDE - 1)
@@ -98,7 +108,7 @@
     def tile_of(target_core, to_z):
         ref = (w_key_ref, w_value_ref)[target_core]
         rows, cols = ((y, x), (x, y))[target_core]
-        return ref.at[pl.ds(pl.multiple_of(rows * 16, 16), 16), pl.ds(pl.multiple_of((cols + to_z) % SIDE * HD, HD), HD)]
+        return ref.at[pl.ds(pl.multiple_of(rows * 16, 16), 16), pl.ds(pl.multiple_of((cols + turn(target_core, to_z)) % SIDE * HD, HD), HD)]
 
     def landing(target_core):
         return weights.at[0, tp, (y, x)[target_core]]
@@ -107,7 +117,7 @@
         to_z = (z + far_first(i)) % Z
         for target_core in range(2):
             pltpu.make_async_remote_copy(
-                tile_of(target_core, to_z), landing(target_core), wz_send, wz_recv,
+                tile_of(target_core, to_z), landing(target_core), wz_send, wz_recv.at[z],
                 device_id=(sp, to_z * 2 + target_core), device_id_type=MESH,
             ).start()
         return carry
@@ -122,7 +132,7 @@
         @pl.when(core != target_core)
         def _():
             pltpu.make_async_remote_copy(
-                tile_of(target_core, z), landing(target_core), wz_send, wz_recv,
+                tile_of(target_core, z), landing(target_core), wz_send, wz_recv.at[z],
                 device_id=(sp, z * 2 + target_core), device_id_type=MESH,
             ).start()
 
@@ -144,36 +154,52 @@
     def sp_of(a, b):
         return a * first_step + b * second_step
 
-    pltpu.make_async_copy(landing(0), landing(0), wl_sem).wait()
-    column = weights.at[0, pl.ds(0, 2 * Z - 1), 0]
+    def pass_on(from_z):
+        tiles = weights.at[0, pl.ds(from_z * 2, 2), first]
+        for i in (2, 1, 3):
+            pltpu.make_async_remote_copy(
+                tiles, tiles, w1_send, w1_recv,
+                device_id=(sp_of((first + i) % SIDE, second), tp), device_id_type=MESH,
+            ).start()
+
+    one, two = weights.at[0, 0, 0], weights.at[0, pl.ds(0, 2), 0]
+
+    def forward(i, carry):
+        from_z = (z + far_first(i)) % Z
+        pltpu.make_async_copy(two, two, wz_recv.at[from_z]).wait()
+        pass_on(from_z)
+        return carry
+
     with jax.named_scope("z_phase"):
-        pltpu.make_async_copy(column, column, wz_recv).wait()
-    strip = weights.at[0, :, first]
-    for i in (1, 3, 2):
-        pltpu.make_async_remote_copy(
-            strip, strip, w1_send, w1_recv,
-            device_id=(sp_of((first + i) % SIDE, second), tp), device_id_type=MESH,
-        ).start()
+        lax.fori_loop(0, Z - 1, forward, 0)
+        pltpu.make_async_copy(one, one, wl_sem).wait()
+        pltpu.make_async_copy(one, one, wz_recv.at[z]).wait()
+        pass_on(z)
     three = weights.at[0, :, pl.ds(0, 3)]
     with jax.named_scope("first_phase"):
         pltpu.make_async_copy(three, three, w1_recv).wait()
-    for i in (1, 3, 2):
+
+    def hand(source, slot, from_slot):
+        target = weights.at[slot, pl.ds(half_of(from_slot), Z)] if slot == 2 else weights.at[slot]
         pltpu.make_async_remote_copy(
-            weights.at[0], weights.at[i], w2_send, w2_recv.at[i],
-            device_id=(sp_of(first, (second + SIDE - i) % SIDE), tp), device_id_type=MESH,
+            source, target, w2_send, w2_recv.at[slot],
+            device_id=(sp_of(first, (second + SIDE + from_slot - slot) % SIDE), tp), device_id_type=MESH,
         ).start()
+
+    for slot in (1, 3):
+        hand(weights.at[0], slot, 0)
 
     half = normed.at[:, 0]
     with jax.named_scope("partner"):
         pltpu.make_async_copy(half, half, x_recv).wait()
 
-    for slot in (0, 1, 3, 2):
-        if slot:
-            with jax.named_scope("slot"):
-                pltpu.make_async_copy(weights.at[slot], weights.at[slot], w2_recv.at[slot]).wait()
-        head = (second + slot + z) % SIDE
-
-        def project(s, carry):
+    def project(slot, i):
+        head = (second + slot + turn(core, z)) % SIDE
+        around = (head + SIDE - z // SIDE) % SIDE
+        odd, back = around % 2, around // 2
+        chip = odd * ((1 - back) * (3 - i) + back * i) + (1 - odd) * (i % 2 * (3 - i // 2) + (1 - i % 2) * (i // 2))
+        for half_at in range(2):
+            s = chip * 2 + (core + half_at) % 2
             raw_rows = jnp.dot(
                 normed[s].reshape(PAIR, D), weights[slot].reshape(D, HD), preferred_element_type=F32
             )
@@ -196,10 +222,21 @@
                         device_id=(sp, target), device_id_type=MESH,
                     ).start()
 
+    for slots in ((0,), (1, 3), (2,)):
+        for slot in slots:
+            if slot:
+                with jax.named_scope("slot"):
+                    pltpu.make_async_copy(weights.at[slot], weights.at[slot], w2_recv.at[slot]).wait()
+            if slot % 2:
+                hand(weights.at[slot, pl.ds(half_of(slot), Z)], 2, slot)
+
+        def project_all(i, carry):
+            for slot in slots:
+                project(slot, i)
             return carry
 
         with jax.named_scope("project"):
-            lax.fori_loop(0, SEQS, project, 0)
+            lax.fori_loop(0, SIDE, project_all, 0)
 
     query = queries[...].astype(BF16)
 
@@ -218,7 +255,7 @@
         lax.fori_loop(0, Z // 2, score, 0)
 
     row = lax.broadcasted_iota(jnp.int32, (1, 8, HD), 1)
-    bias = jnp.where(row == 0, bias_ref[group * 2], bias_ref[group * 2 + 1])
+    bias = jnp.where(row % 2 == 0, bias_ref[group * 2], bias_ref[group * 2 + 1])
     score_all = scores[...] * (HD ** -0.5) + bias
     soft = log1p_unit(jnp.exp(-jnp.abs(score_all)))
     log_keep = -(jnp.maximum(score_all, 0.0) + soft)
@@ -249,8 +286,7 @@
             chunk_weights[chunk], value_out[0, pl.ds(chunk * HD, HD), :], preferred_element_type=F32
         )
 
-    parts[sp, pl.ds(0, 8), :] = partial
-    parts[sp, pl.ds(8, 8), :] = jnp.broadcast_to(carried, (8, HD))
+    parts[sp] = jnp.where(row[0] < 2, partial, carried)
 
     def share(i, carry):
         pltpu.make_async_remote_copy(
@@ -263,14 +299,7 @@
     others = parts.at[pl.ds(0, SIDE * SIDE - 1)]
     with jax.named_scope("others"):
         pltpu.make_async_copy(others, others, p_recv).wait()
-    total = jnp.zeros((8, HD), F32)
-    log_later = jnp.zeros((8, HD), F32)
-    for span in reversed(range(SIDE * SIDE)):
-        total = total + jnp.exp(log_later) * parts[span, pl.ds(0, 8), :]
-        log_later = log_later + parts[span, pl.ds(8, 8), :]
-    read_out[:, pl.ds(0, HD)] = total[0:1]
-    read_out[:, pl.ds(HD, HD)] = total[1:2]
-
+    column = weights.at[0, pl.ds(0, 2 * Z - 1), 0]
     pltpu.make_async_copy(column, column, wz_send).wait()
     pltpu.make_async_copy(three, three, w1_send).wait()
     pltpu.make_async_copy(weights.at[pl.ds(0, 3)], weights.at[pl.ds(0, 3)], w2_send).wait()
@@ -282,16 +311,38 @@
     pltpu.make_async_copy(others, others, p_send).wait()
 
 
+def write_out(key_ref, value_ref, parts_ref, key_out, value_out, read_out, read, sems):
+    copies = [
+        pltpu.make_async_copy(ref.at[0, pl.ds(i * (SPAN // 4), SPAN // 4)], out.at[0, pl.ds(i * (SPAN // 4), SPAN // 4)], sems.at[n, i])
+        for n, (ref, out) in enumerate(((key_ref, key_out), (value_ref, value_out)))
+        for i in range(4)
+    ]
+    for copy in copies:
+        copy.start()
+    total = jnp.zeros((2, HD), F32)
+    log_later = jnp.zeros((2, HD), F32)
+    for span in reversed(range(SIDE * SIDE)):
+        total = total + jnp.exp(log_later) * parts_ref[span, pl.ds(0, 2), :]
+        log_later = log_later + parts_ref[span, pl.ds(2, 2), :]
+    read[:, pl.ds(0, HD)] = total[0:1]
+    read[:, pl.ds(HD, HD)] = total[1:2]
+    last = pltpu.make_async_copy(read, read_out, sems.at[2, 0])
+    last.start()
+    for copy in copies:
+        copy.wait()
+    last.wait()
+
+
 def shards(tokens, in_gain, w_key, w_value, k_gain, new_query, q_gain, stick_bias):
     vmem = pl.BlockSpec(memory_space=pltpu.VMEM)
     hbm = pl.BlockSpec(memory_space=pltpu.HBM)
     dma = pltpu.SemaphoreType.DMA
-    return pl.pallas_call(
+    key_rows, value_rows, parts = pl.pallas_call(
         kernel,
         out_shape=(
             jax.ShapeDtypeStruct((1, SPAN, HD), BF16),
             jax.ShapeDtypeStruct((1, SPAN, HD), BF16),
-            jax.ShapeDtypeStruct((1, 2 * HD), F32),
+            jax.ShapeDtypeStruct((SIDE * SIDE, 8, HD), F32),
         ),
         in_specs=[hbm] * 8,
         out_specs=(vmem, vmem, vmem),
@@ -310,8 +361,7 @@
             pltpu.VMEM((CHUNKS, 8, HD), F32),
             pltpu.VMEM((16, HD), F32),
             pltpu.VMEM((8, SEQS, HD), F32),
-            pltpu.VMEM((SIDE * SIDE, 16, HD), F32),
-            dma((7,)), dma((SEQS,)), dma, dma, dma, dma, dma, dma, dma((SIDE,)), dma, dma,
+            dma((7,)), dma((SEQS,)), dma, dma((Z,)), dma, dma, dma, dma, dma((SIDE,)), dma, dma,
             dma, dma((2, Z)), dma, dma,
         ],
         compiler_params=pltpu.CompilerParams(
@@ -326,6 +376,18 @@
             )
         )
     )
+    return pl.pallas_call(
+        write_out,
+        out_shape=(
+            jax.ShapeDtypeStruct((1, SPAN, HD), BF16),
+            jax.ShapeDtypeStruct((1, SPAN, HD), BF16),
+            jax.ShapeDtypeStruct((1, 2 * HD), F32),
+        ),
+        in_specs=[vmem] * 3,
+        out_specs=[hbm] * 3,
+        scratch_shapes=[pltpu.VMEM((1, 2 * HD), F32), dma((3, 4))],
+        compiler_params=pltpu.CompilerParams(vmem_limit_bytes=40 * 2**20),
+    )(key_rows, value_rows, parts)
 
 
 def solution(mesh):

time: 117 us -> 115 us (0.983)
  the two profiles are of different devices: /device:TPU:97 before, /device:TPU:1 now
where the time goes in v3:
time: 115 us
  Pallas kernels  114 us (99%)
    pallas_call x1, Pallas kernels, shards(): pl.pallas_call(kernel, out_shape=(jax.ShapeDtypeStruct((1, SPAN, HD), BF1...  113 us

profile of v3, /device:TPU:1, one launch (start us, length us, event | category | flops | bytes accessed | tf_op | source)
XLA Modules:
  0.0 114.8 jit_solution(16081428398466972972)
XLA Ops:
  0.6 112.9 %shard_map.103 = (bf16[1,3072,128]{2,1,0:T(8,128)(2,1)S(1)}, bf16[1,3072,128]{2,1,0:T(8,128)(2,1)S(1)}, f32[16,8,128]{2,1,0:T(8,128)S(1)}) custom-call(bf16[8,96,2048]{2,1,0:T(8,128)(2,1)} %tokens_ref.1, f32[1,2048]{1,0:T(1,128)} %bitcast.3, bf16[64,512]{1,0:T(8,128)(2,1)} %w_key_in.1, bf16[64,512]{1,0:T(8,128)(2,1)} %w_value_in.1, f32[1,128]{1,0:T(1,128)} %bitcast.4, ...), custom_call_target="tpu_custom_call" | custom-call | tf_op jit(solution)/shard_map/pallas_call | solution.py:340
  113.5 1.2 %shard_map.104 = (bf16[1,3072,128]{2,1,0:T(8,128)(2,1)}, bf16[1,3072,128]{2,1,0:T(8,128)(2,1)}, f32[1,256]{1,0:T(1,128)}) custom-call(bf16[1,3072,128]{2,1,0:T(8,128)(2,1)S(1)} %get-tuple-element.6.key_ref, bf16[1,3072,128]{2,1,0:T(8,128)(2,1)S(1)} %get-tuple-element.7.value_ref, f32[16,8,128]{2,1,0:T(8,128)S(1)} %get-tuple-element.8.parts_ref), custom_call_target="tpu_custom_call" | custom-call | tf_op jit(solution)/shard_map/pallas_call | solution.py:379

commit v4 on v3

--- a/solution.py
+++ b/solution.py
@@ -32,8 +32,8 @@
     return 2.0 * t * (acc * t2 + 1.0)
 
 
-def turn(target_core, chip_z):
-    return chip_z // SIDE + (chip_z + target_core * (Z - 2 * chip_z))
+def first_head(second, chip_z, target_core):
+    return (second + chip_z // SIDE + chip_z + target_core * 2 * (Z - chip_z)) % SIDE
 
 
 def half_of(slot):
@@ -107,24 +107,24 @@
 
     def tile_of(target_core, to_z):
         ref = (w_key_ref, w_value_ref)[target_core]
-        rows, cols = ((y, x), (x, y))[target_core]
-        return ref.at[pl.ds(pl.multiple_of(rows * 16, 16), 16), pl.ds(pl.multiple_of((cols + turn(target_core, to_z)) % SIDE * HD, HD), HD)]
+        rows, head = (y, x)[target_core], first_head((x, y)[target_core], to_z, target_core)
+        return ref.at[pl.ds(pl.multiple_of(rows * 16, 16), 16), pl.ds(pl.multiple_of(head * HD, HD), HD)]
 
     def landing(target_core):
         return weights.at[0, tp, (y, x)[target_core]]
 
-    def deal(i, carry):
+    def deal(target_core, i, carry):
         to_z = (z + far_first(i)) % Z
-        for target_core in range(2):
-            pltpu.make_async_remote_copy(
-                tile_of(target_core, to_z), landing(target_core), wz_send, wz_recv.at[z],
-                device_id=(sp, to_z * 2 + target_core), device_id_type=MESH,
-            ).start()
-        return carry
-
-    with jax.named_scope("deal"):
-        lax.fori_loop(0, Z - 1, deal, 0)
-    for target_core in range(2):
+        pltpu.make_async_remote_copy(
+            tile_of(target_core, to_z), landing(target_core), wz_send, wz_recv.at[z],
+            device_id=(sp, to_z * 2 + target_core), device_id_type=MESH,
+        ).start()
+        return carry
+
+    def deal_all(target_core):
+        with jax.named_scope("deal"):
+            lax.fori_loop(0, Z - 1, functools.partial(deal, target_core), 0)
+
         @pl.when(core == target_core)
         def _():
             pltpu.make_async_copy(tile_of(target_core, z), landing(target_core), wl_sem).start()
@@ -135,6 +135,8 @@
                 tile_of(target_core, z), landing(target_core), wz_send, wz_recv.at[z],
                 device_id=(sp, z * 2 + target_core), device_id_type=MESH,
             ).start()
+
+    deal_all(0)
 
     def norm(s, carry):
         pltpu.make_async_copy(tokens_ref.at[s], raw.at[s], tok_sem.at[s]).wait()
@@ -151,6 +153,8 @@
     with jax.named_scope("norm"):
         lax.fori_loop(0, SEQS, norm, 0)
 
+    deal_all(1)
+
     def sp_of(a, b):
         return a * first_step + b * second_step
 
@@ -165,16 +169,16 @@
     one, two = weights.at[0, 0, 0], weights.at[0, pl.ds(0, 2), 0]
 
     def forward(i, carry):
-        from_z = (z + far_first(i)) % Z
+        from_z = (z + far_first(Z - 2 - i)) % Z
         pltpu.make_async_copy(two, two, wz_recv.at[from_z]).wait()
         pass_on(from_z)
         return carry
 
     with jax.named_scope("z_phase"):
-        lax.fori_loop(0, Z - 1, forward, 0)
         pltpu.make_async_copy(one, one, wl_sem).wait()
         pltpu.make_async_copy(one, one, wz_recv.at[z]).wait()
         pass_on(z)
+        lax.fori_loop(0, Z - 1, forward, 0)
     three = weights.at[0, :, pl.ds(0, 3)]
     with jax.named_scope("first_phase"):
         pltpu.make_async_copy(three, three, w1_recv).wait()
@@ -194,7 +198,7 @@
         pltpu.make_async_copy(half, half, x_recv).wait()
 
     def project(slot, i):
-        head = (second + slot + turn(core, z)) % SIDE
+        head = (first_head(second, z, core) + slot) % SIDE
         around = (head + SIDE - z // SIDE) % SIDE
         odd, back = around % 2, around // 2
         chip = odd * ((1 - back) * (3 - i) + back * i) + (1 - odd) * (i % 2 * (3 - i // 2) + (1 - i % 2) * (i // 2))
@@ -222,21 +226,40 @@
                         device_id=(sp, target), device_id_type=MESH,
                     ).start()
 
-    for slots in ((0,), (1, 3), (2,)):
-        for slot in slots:
-            if slot:
-                with jax.named_scope("slot"):
-                    pltpu.make_async_copy(weights.at[slot], weights.at[slot], w2_recv.at[slot]).wait()
-            if slot % 2:
-                hand(weights.at[slot, pl.ds(half_of(slot), Z)], 2, slot)
-
-        def project_all(i, carry):
-            for slot in slots:
-                project(slot, i)
-            return carry
-
+    def project_slot(slot, n, carry):
+        project(slot, n)
+        return carry
+
+    with jax.named_scope("project"):
+        lax.fori_loop(0, SIDE, functools.partial(project_slot, 0), 0)
+    for slot in (1, 3):
+        with jax.named_scope("slot"):
+            pltpu.make_async_copy(weights.at[slot], weights.at[slot], w2_recv.at[slot]).wait()
+        hand(weights.at[slot, pl.ds(half_of(slot), Z)], 2, slot)
+
+    off = (first_head(second, z, core) + SIDE - z // SIDE) % SIDE
+    odd, upper = off % 2, off // 2
+
+    def third(turn, n, carry):
+        both_slot, both_at = 1 + 2 * (n % 2), n // 2
+        if turn == 0:
+            slot, at = odd * off + (1 - odd) * both_slot, odd * n + (1 - odd) * both_at
+        elif turn == 1:
+            both = (1 - odd) * upper
+            slot, at = both * both_slot + (1 - both) * 2, both * (both_at + 2) + (1 - both) * n
+        else:
+            both, two = (1 - odd) * (1 - upper), (1 - odd) * upper
+            slot = both * both_slot + two * 2 + odd * (SIDE - off)
+            at = both * (both_at + 2) + (1 - both) * n
+        project(slot, at)
+        return carry
+
+    for turn in range(3):
+        if turn == 1:
+            with jax.named_scope("slot"):
+                pltpu.make_async_copy(weights.at[2], weights.at[2], w2_recv.at[2]).wait()
         with jax.named_scope("project"):
-            lax.fori_loop(0, SIDE, project_all, 0)
+            lax.fori_loop(0, SIDE, functools.partial(third, turn), 0)
 
     query = queries[...].astype(BF16)
 

time: 115 us -> 109 us (0.948)
  Pallas kernels: 114 us -> 109 us
    pallas_call x1, Pallas kernels: 113 us -> 107 us  [shards(): pl.pallas_call(kernel, out_shape=(jax.ShapeDtypeStruct((1, SPAN, HD), BF1...]
where the time goes in v4:
time: 109 us
  Pallas kernels  109 us (100%)
    pallas_call x1, Pallas kernels, shards(): pl.pallas_call(kernel, out_shape=(jax.ShapeDtypeStruct((1, SPAN, HD), BF1...  107 us

profile of v4, /device:TPU:1, one launch (start us, length us, event | category | flops | bytes accessed | tf_op | source)
XLA Modules:
  0.0 109.2 jit_solution(6707990540870418215)
XLA Ops:
  0.6 107.3 %shard_map.103 = (bf16[1,3072,128]{2,1,0:T(8,128)(2,1)S(1)}, bf16[1,3072,128]{2,1,0:T(8,128)(2,1)S(1)}, f32[16,8,128]{2,1,0:T(8,128)S(1)}) custom-call(bf16[8,96,2048]{2,1,0:T(8,128)(2,1)} %tokens_ref.1, f32[1,2048]{1,0:T(1,128)} %bitcast.3, bf16[64,512]{1,0:T(8,128)(2,1)} %w_key_in.1, bf16[64,512]{1,0:T(8,128)(2,1)} %w_value_in.1, f32[1,128]{1,0:T(1,128)} %bitcast.4, ...), custom_call_target="tpu_custom_call" | custom-call | tf_op jit(solution)/shard_map/pallas_call | solution.py:363
  108.0 1.2 %shard_map.104 = (bf16[1,3072,128]{2,1,0:T(8,128)(2,1)}, bf16[1,3072,128]{2,1,0:T(8,128)(2,1)}, f32[1,256]{1,0:T(1,128)}) custom-call(bf16[1,3072,128]{2,1,0:T(8,128)(2,1)S(1)} %get-tuple-element.6.key_ref, bf16[1,3072,128]{2,1,0:T(8,128)(2,1)S(1)} %get-tuple-element.7.value_ref, f32[16,8,128]{2,1,0:T(8,128)S(1)} %get-tuple-element.8.parts_ref), custom_call_target="tpu_custom_call" | custom-call | tf_op jit(solution)/shard_map/pallas_call | solution.py:402

commit v5 on v4

--- a/solution.py
+++ b/solution.py
@@ -179,19 +179,22 @@
         pltpu.make_async_copy(one, one, wz_recv.at[z]).wait()
         pass_on(z)
         lax.fori_loop(0, Z - 1, forward, 0)
-    three = weights.at[0, :, pl.ds(0, 3)]
-    with jax.named_scope("first_phase"):
-        pltpu.make_async_copy(three, three, w1_recv).wait()
-
-    def hand(source, slot, from_slot):
-        target = weights.at[slot, pl.ds(half_of(from_slot), Z)] if slot == 2 else weights.at[slot]
+
+    def hand(source, target, slot, from_slot):
         pltpu.make_async_remote_copy(
             source, target, w2_send, w2_recv.at[slot],
             device_id=(sp_of(first, (second + SIDE + from_slot - slot) % SIDE), tp), device_id_type=MESH,
         ).start()
 
     for slot in (1, 3):
-        hand(weights.at[0], slot, 0)
+        hand(weights.at[0, :, first], weights.at[slot, :, first], slot, 0)
+    three = weights.at[0, :, pl.ds(0, 3)]
+    with jax.named_scope("first_phase"):
+        pltpu.make_async_copy(three, three, w1_recv).wait()
+    for i in range(1, SIDE):
+        rows = (first + i) % SIDE
+        for slot in (1, 3):
+            hand(weights.at[0, :, rows], weights.at[slot, :, rows], slot, 0)
 
     half = normed.at[:, 0]
     with jax.named_scope("partner"):
@@ -202,14 +205,15 @@
         around = (head + SIDE - z // SIDE) % SIDE
         odd, back = around % 2, around // 2
         chip = odd * ((1 - back) * (3 - i) + back * i) + (1 - odd) * (i % 2 * (3 - i // 2) + (1 - i % 2) * (i // 2))
+        both = pl.ds(chip * 2, 2)
+        raw_rows = jnp.dot(
+            normed[both].reshape(2 * PAIR, D), weights[slot].reshape(D, HD), preferred_element_type=F32
+        )
+        inverse = lax.rsqrt(jnp.mean(raw_rows * raw_rows, axis=-1, keepdims=True) + NORM_EPS)
+        out = jnp.where(core == 0, raw_rows * inverse * k_gain_ref[...], raw_rows)
+        sendbuf[pl.ds(slot * SEQS + chip * 2, 2)] = out.astype(BF16).reshape(2, PAIR, HD)
         for half_at in range(2):
             s = chip * 2 + (core + half_at) % 2
-            raw_rows = jnp.dot(
-                normed[s].reshape(PAIR, D), weights[slot].reshape(D, HD), preferred_element_type=F32
-            )
-            inverse = lax.rsqrt(jnp.mean(raw_rows * raw_rows, axis=-1, keepdims=True) + NORM_EPS)
-            out = jnp.where(core == 0, raw_rows * inverse * k_gain_ref[...], raw_rows)
-            sendbuf[slot * SEQS + s] = out.astype(BF16)
             target = head * SEQS + s
             source = sendbuf.at[slot * SEQS + s]
             for which, out_ref in enumerate((key_out, value_out)):
@@ -235,7 +239,8 @@
     for slot in (1, 3):
         with jax.named_scope("slot"):
             pltpu.make_async_copy(weights.at[slot], weights.at[slot], w2_recv.at[slot]).wait()
-        hand(weights.at[slot, pl.ds(half_of(slot), Z)], 2, slot)
+        half_rows = pl.ds(half_of(slot), Z)
+        hand(weights.at[slot, half_rows], weights.at[2, half_rows], 2, slot)
 
     off = (first_head(second, z, core) + SIDE - z // SIDE) % SIDE
     odd, upper = off % 2, off // 2

time: 109 us -> 109 us (level)
  no operation moved by 1% of the time
where the time goes in v5:
time: 109 us
  Pallas kernels  108 us (99%)
    pallas_call x1, Pallas kernels, shards(): pl.pallas_call(kernel, out_shape=(jax.ShapeDtypeStruct((1, SPAN, HD), BF1...  107 us

profile of v5, /device:TPU:1, one launch (start us, length us, event | category | flops | bytes accessed | tf_op | source)
XLA Modules:
  0.0 108.8 jit_solution(14539223179484199955)
XLA Ops:
  0.6 107.0 %shard_map.103 = (bf16[1,3072,128]{2,1,0:T(8,128)(2,1)S(1)}, bf16[1,3072,128]{2,1,0:T(8,128)(2,1)S(1)}, f32[16,8,128]{2,1,0:T(8,128)S(1)}) custom-call(bf16[8,96,2048]{2,1,0:T(8,128)(2,1)} %tokens_ref.1, f32[1,2048]{1,0:T(1,128)} %bitcast.3, bf16[64,512]{1,0:T(8,128)(2,1)} %w_key_in.1, bf16[64,512]{1,0:T(8,128)(2,1)} %w_value_in.1, f32[1,128]{1,0:T(1,128)} %bitcast.4, ...), custom_call_target="tpu_custom_call" | custom-call | tf_op jit(solution)/shard_map/pallas_call | solution.py:368
  107.6 1.2 %shard_map.104 = (bf16[1,3072,128]{2,1,0:T(8,128)(2,1)}, bf16[1,3072,128]{2,1,0:T(8,128)(2,1)}, f32[1,256]{1,0:T(1,128)}) custom-call(bf16[1,3072,128]{2,1,0:T(8,128)(2,1)S(1)} %get-tuple-element.6.key_ref, bf16[1,3072,128]{2,1,0:T(8,128)(2,1)S(1)} %get-tuple-element.7.value_ref, f32[16,8,128]{2,1,0:T(8,128)S(1)} %get-tuple-element.8.parts_ref), custom_call_target="tpu_custom_call" | custom-call | tf_op jit(solution)/shard_map/pallas_call | solution.py:407

commit v6 on v5

--- a/solution.py
+++ b/solution.py
@@ -296,23 +296,23 @@
     ).reshape(CHUNKS, 8, HD)
     totals = jnp.sum(log_keep, axis=2, keepdims=True)
     carried = jnp.zeros((8, 1), F32)
-    chunk_weights = [None] * CHUNKS
     for chunk in reversed(range(CHUNKS)):
-        chunk_weights[chunk] = jnp.exp(log_take[chunk] + after[chunk] + carried).astype(BF16)
+        scores[chunk] = jnp.exp(log_take[chunk] + after[chunk] + carried)
         carried = carried + totals[chunk]
 
-    def arrive(at, carry):
-        block = value_out.at[0, pl.ds(pl.multiple_of(at * PAIR, PAIR), PAIR)]
-        pltpu.make_async_copy(block, block, kv_recv.at[1, at]).wait()
-        return carry
+    def read_pair(pair, partial):
+        for i in range(2):
+            at = pair * 2 + i
+            block = value_out.at[0, pl.ds(pl.multiple_of(at * PAIR, PAIR), PAIR)]
+            pltpu.make_async_copy(block, block, kv_recv.at[1, at]).wait()
+        for i in range(3):
+            chunk = pair * 3 + i
+            values = value_out[0, pl.ds(pl.multiple_of(chunk * HD, HD), HD), :]
+            partial = partial + jnp.dot(scores[chunk].astype(BF16), values, preferred_element_type=F32)
+        return partial
 
     with jax.named_scope("arrive"):
-        lax.fori_loop(0, Z, arrive, 0)
-    partial = jnp.zeros((8, HD), F32)
-    for chunk in range(CHUNKS):
-        partial = partial + jnp.dot(
-            chunk_weights[chunk], value_out[0, pl.ds(chunk * HD, HD), :], preferred_element_type=F32
-        )
+        partial = lax.fori_loop(0, Z // 2, read_pair, jnp.zeros((8, HD), F32))
 
     parts[sp] = jnp.where(row[0] < 2, partial, carried)
 

time: 109 us -> 109 us (level)
  no operation moved by 1% of the time
where the time goes in v6:
time: 109 us
  Pallas kernels  109 us (100%)
    pallas_call x1, Pallas kernels, shards(): pl.pallas_call(kernel, out_shape=(jax.ShapeDtypeStruct((1, SPAN, HD), BF1...  107 us

profile of v6, /device:TPU:1, one launch (start us, length us, event | category | flops | bytes accessed | tf_op | source)
XLA Modules:
  0.0 109.4 jit_solution(2580032500451129517)
XLA Ops:
  0.6 107.5 %shard_map.103 = (bf16[1,3072,128]{2,1,0:T(8,128)(2,1)S(1)}, bf16[1,3072,128]{2,1,0:T(8,128)(2,1)S(1)}, f32[16,8,128]{2,1,0:T(8,128)S(1)}) custom-call(bf16[8,96,2048]{2,1,0:T(8,128)(2,1)} %tokens_ref.1, f32[1,2048]{1,0:T(1,128)} %bitcast.3, bf16[64,512]{1,0:T(8,128)(2,1)} %w_key_in.1, bf16[64,512]{1,0:T(8,128)(2,1)} %w_value_in.1, f32[1,128]{1,0:T(1,128)} %bitcast.4, ...), custom_call_target="tpu_custom_call" | custom-call | tf_op jit(solution)/shard_map/pallas_call | solution.py:368
  108.1 1.2 %shard_map.104 = (bf16[1,3072,128]{2,1,0:T(8,128)(2,1)}, bf16[1,3072,128]{2,1,0:T(8,128)(2,1)}, f32[1,256]{1,0:T(1,128)}) custom-call(bf16[1,3072,128]{2,1,0:T(8,128)(2,1)S(1)} %get-tuple-element.6.key_ref, bf16[1,3072,128]{2,1,0:T(8,128)(2,1)S(1)} %get-tuple-element.7.value_ref, f32[16,8,128]{2,1,0:T(8,128)S(1)} %get-tuple-element.8.parts_ref), custom_call_target="tpu_custom_call" | custom-call | tf_op jit(solution)/shard_map/pallas_call | solution.py:407
